TPU v7x, 32 devices: a whole 2x2x4 slice. The times are simulated.
32 devices in a mesh: ep: 8 (over z, core), tp: 4 (over y, x).
Axes of the slice: x: 2, y: 2, z: 4, core: 2. Of those that a mesh axis runs over, the one named last changes fastest.
Arguments:
- mix_in: bfloat16 [2048, 2048], P('ep'), may hold values from -6 to 6
- mix_gain: float32 [2048], replicated, may hold values from 0.1 to 1.9
- w_in_x: bfloat16 [2048, 2048], P(None, 'tp'), may hold values from -0.125 to 0.125
- w_in_y: bfloat16 [2048, 2048], P(None, 'tp'), may hold values from -0.125 to 0.125
- conv_taps: float32 [4, 2048], P(None, 'tp'), may hold values from -3 to 3
- recur_gate_w: bfloat16 [16, 128, 128], P('tp'), may hold values from -0.5 to 0.5
- input_gate_w: bfloat16 [16, 128, 128], P('tp'), may hold values from -0.5 to 0.5
- decay_logit: float32 [2048], P('tp'), may hold values from 4 to 20
- decay_shift: float32 [2048, 2048], P('ep', 'tp'), may hold values from -2.2 to 0
- moe_in: bfloat16 [2048, 2048], P('ep'), may hold values from -6 to 6
- moe_gain: float32 [2048], replicated, may hold values from 0.1 to 1.9
- routes: int32 [2048, 2], P('ep'), may hold values from 0 to 7, all different within a row; in each aligned block of 256 rows (0 to 255, 256 to 511, ...) at most 128 rows name the same one
- route_weight: float32 [2048, 2], P('ep'), may hold values from 0.1 to 1
- expert_gate: bfloat16 [8, 2048, 2048], P('ep', None, 'tp'), may hold values from -0.125 to 0.125
- expert_up: bfloat16 [8, 2048, 2048], P('ep', None, 'tp'), may hold values from -0.125 to 0.125
- expert_down: bfloat16 [8, 2048, 2048], P('ep', None, 'tp'), may hold values from -0.125 to 0.125
Outputs:
- mixer_out: bfloat16 [2048, 2048], P('ep', 'tp')
- moe_out: bfloat16 [2048, 2048], P('ep', 'tp')
Inputs may be any that keep to these rules, and one draw needn't show every extreme that they name: `routes`: each row names 2 different experts. Among the rows of one index of ep no expert is named more than 128 times, a bound that some block reaches.
All inputs are finite; a program needn't handle non-finite values.
Results may differ from a plain program's by a relative error of at most 0.0095.
Values may be sent and summed in bfloat16 or wider, within the bound.
A program may use at most 64 MiB of HBM per device.

v0:
```python
import jax
import jax.numpy as jnp
from jax import lax
from jax.sharding import PartitionSpec as P

epsilon = 1e-06
lru_scale = 8.0


def from_behind(value, axis, by):
    count = lax.axis_size(axis)
    pairs = [(i, i + by) for i in range(count) if 0 <= i + by < count]
    return lax.ppermute(value, axis, pairs)


def entering(value, axis, combine, identity):
    count, index = (lax.axis_size(axis), lax.axis_index(axis))
    everything = jax.tree.map(lambda part: lax.all_gather(part, axis), value)
    start = jax.tree.map(
        lambda part, zero: jnp.broadcast_to(jnp.asarray(zero, part.dtype), part.shape),
        value,
        identity,
    )

    def hop(k, before):
        reached = k < index
        new = combine(before, jax.tree.map(lambda part: part[k], everything))
        return jax.tree.map(lambda a, b: jnp.where(reached, a, b), new, before)

    return lax.fori_loop(0, count, hop, start)


def norm_rows(rows, gain):
    widened = rows.astype(jnp.float32)
    scaled = widened * lax.rsqrt(jnp.mean(widened * widened, axis=-1, keepdims=True) + epsilon)
    return (scaled * gain[None, :]).astype(jnp.bfloat16)


def link(earlier, later):
    return (earlier[0] * later[0], later[0] * earlier[1] + later[1])


def local(
    mix_in,
    mix_gain,
    w_in_x,
    w_in_y,
    conv_taps,
    recur_gate_w,
    input_gate_w,
    decay_logit,
    decay_shift,
    moe_in,
    moe_gain,
    routes,
    route_weight,
    expert_gate,
    expert_up,
    expert_down,
):
    row_count = mix_in.shape[0]
    width_dev = w_in_x.shape[1]
    heads_dev = recur_gate_w.shape[0]
    block_size = recur_gate_w.shape[1]
    tap_count = conv_taps.shape[0]
    mixer_rows = norm_rows(mix_in, mix_gain)
    x_branch = jnp.dot(mixer_rows, w_in_x, preferred_element_type=jnp.float32).astype(jnp.bfloat16)
    y_branch = jnp.dot(mixer_rows, w_in_y, preferred_element_type=jnp.float32).astype(jnp.bfloat16)
    previous = from_behind(x_branch[row_count - (tap_count - 1) :], "ep", 1)
    padded = jnp.concatenate([previous, x_branch], axis=0)
    conv_sum = jnp.zeros((row_count, width_dev), jnp.float32)
    for tap_index in range(tap_count):
        conv_sum = conv_sum + conv_taps[tap_index][None, :] * padded[
            tap_index : tap_index + row_count
        ].astype(jnp.float32)
    x_conv = conv_sum.astype(jnp.bfloat16)
    heads_in = x_conv.reshape(row_count, heads_dev, block_size)
    gate_a = jnp.einsum(
        "thi,hij->thj", heads_in, recur_gate_w, preferred_element_type=jnp.float32
    ).reshape(row_count, width_dev)
    gate_x = jnp.einsum(
        "thi,hij->thj", heads_in, input_gate_w, preferred_element_type=jnp.float32
    ).reshape(row_count, width_dev)
    log_decay = (
        -lru_scale * jax.nn.sigmoid(gate_a) * jax.nn.softplus(-decay_logit)[None, :] + decay_shift
    )
    lru_drive = (
        jnp.sqrt(-jnp.expm1(2.0 * log_decay)) * jax.nn.sigmoid(gate_x) * x_conv.astype(jnp.float32)
    )
    through, local_state = lax.associative_scan(link, (jnp.exp(log_decay), lru_drive), axis=0)
    identity = (jnp.ones((width_dev,), jnp.float32), jnp.zeros((width_dev,), jnp.float32))
    carried = entering((through[row_count - 1], local_state[row_count - 1]), "ep", link, identity)
    lru_state = local_state + through * carried[1][None, :]
    mixer_out = (lru_state * jax.nn.gelu(y_branch.astype(jnp.float32))).astype(jnp.bfloat16)
    moe_rows = norm_rows(moe_in, moe_gain)
    token_count = moe_rows.shape[0]
    feature_count = moe_rows.shape[1]
    choose_count = routes.shape[1]
    expert_count = lax.axis_size("ep")
    capacity = 2 * token_count * choose_count // expert_count
    slot_total = expert_count * capacity
    expert_ids = routes.reshape(-1)
    onehot = (expert_ids[:, None] == jnp.arange(expert_count, dtype=jnp.int32)[None, :]).astype(
        jnp.int32
    )
    slot_rank = jnp.sum(jnp.cumsum(onehot, axis=0) * onehot, axis=1) - 1
    slot_index = expert_ids * capacity + slot_rank
    token_index = jnp.repeat(jnp.arange(token_count, dtype=jnp.int32), choose_count)
    slot_owner = jnp.full((slot_total,), token_count, jnp.int32).at[slot_index].set(token_index)
    padded_rows = jnp.concatenate([moe_rows, jnp.zeros((1, feature_count), jnp.bfloat16)], axis=0)
    outgoing = padded_rows[slot_owner].reshape(expert_count, capacity, feature_count)
    column_width = feature_count // lax.axis_size("tp")
    own_columns = lax.dynamic_slice_in_dim(
        outgoing, lax.axis_index("tp") * column_width, column_width, 2
    )
    incoming = lax.all_to_all(own_columns, "ep", split_axis=0, concat_axis=0, tiled=True)
    piece = lax.all_gather(incoming, "tp", axis=2, tiled=True)
    flat_rows = piece.reshape(slot_total, piece.shape[2])
    gate_rows = expert_gate[0]
    up_rows = expert_up[0]
    gate_proj = jnp.dot(flat_rows, gate_rows, preferred_element_type=jnp.float32)
    up_proj = jnp.dot(flat_rows, up_rows, preferred_element_type=jnp.float32)
    hidden = (jax.nn.silu(gate_proj) * up_proj).astype(jnp.bfloat16)
    down_rows = expert_down[0]
    columns = jnp.dot(
        lax.all_gather(hidden, "tp", axis=1, tiled=True),
        down_rows,
        preferred_element_type=jnp.float32,
    )
    results = columns.astype(jnp.bfloat16).reshape(expert_count, capacity, expert_down.shape[2])
    returned = lax.all_to_all(results, "ep", split_axis=0, concat_axis=0, tiled=True).reshape(
        slot_total, expert_down.shape[2]
    )
    picked = (
        returned[slot_index]
        .astype(jnp.float32)
        .reshape(token_count, choose_count, expert_down.shape[2])
    )
    route_share = route_weight / jnp.sum(route_weight, axis=1, keepdims=True)
    moe_out = jnp.sum(route_share[:, :, None] * picked, axis=1).astype(jnp.bfloat16)
    return (mixer_out, moe_out)


def solution(mesh):
    placed = (
        P("ep", None),
        P(),
        P(None, "tp"),
        P(None, "tp"),
        P(None, "tp"),
        P("tp", None, None),
        P("tp", None, None),
        P("tp"),
        P("ep", "tp"),
        P("ep", None),
        P(),
        P("ep", None),
        P("ep", None),
        P("ep", None, "tp"),
        P("ep", None, "tp"),
        P("ep", None, "tp"),
    )
    return jax.shard_map(
        local, mesh=mesh, in_specs=placed, out_specs=(P("ep", "tp"), P("ep", "tp")), check_vma=False
    )
```

profile of v0, /device:TPU:0, one launch (start us, length us, event | category | flops | bytes accessed | tf_op | source)
XLA Modules:
  0.0 283.7 jit_solution(14209495019624665678)
XLA Ops:
  11.2 2.4 scatter_custom_fusion
  15.6 6.0 %gather_fusion = bf16[1024,2048]{1,0:T(8,128)(2,1)} fusion(bf16[257,2048]{1,0:T(8,128)(2,1)S(1)} %concatenate.63, s32[1024]{0:T(1024)S(1)} %fusion.50), kind=kCustom, calls=%fused_computation | custom fusion | bytes 8392704 | tf_op jit(solution)/shard_map/gather | solution.py:111
  22.9 33.0 %all_to_all.10 = bf16[8,128,512]{2,1,0:T(8,128)(2,1)} all-to-all(bf16[8,128,512]{2,1,0:T(8,128)(2,1)S(1)} %constant_dynamic-slice_fusion.2), channel_id=1, replica_groups=mesh['ep'=8,'tp'=4] {'ep'}, dimensions={0} | all-to-all | bytes 2097152 | tf_op jit(solution)/shard_map/all_to_all | solution.py:116
  56.8 2.4 convolution_convert_fusion.1
  59.9 1.5 collective-permute-start
  63.0 1.7 add_convert_fusion
  64.7 42.8 %all-gather.5.cloned.1.call-done = bf16[8,128,2048]{2,1,0:T(8,128)(2,1)} async-done(((bf16[8,128,512]{2,1,0:T(8,128)(2,1)}), bf16[8,128,2048]{2,1,0:T(8,128)(2,1)}) %all-gather.5.cloned.1.call-update) | async-done | bytes 4194320 | tf_op jit(solution)/shard_map/all_gather | solution.py:117
  107.4 4.7 %fusion.8 = f32[1024,512]{1,0:T(8,128)S(1)} fusion(bf16[1024,2048]{1,0:T(8,128)(2,1)} %bitcast.86, bf16[1,2048,512]{2,1,0:T(8,128)(2,1)S(1)} %copy-done), kind=kOutput, calls=%fused_computation.18 | convolution fusion | flops 2147483648 | bytes 8388608 | tf_op jit(solution)/shard_map/dot_general | solution.py:122
  112.1 3.7 %multiply_convert_fusion = bf16[1024,512]{1,0:T(8,128)(2,1)} fusion(f32[1024,512]{1,0:T(8,128)S(1)} %fusion.8, bf16[1024,2048]{1,0:T(8,128)(2,1)S(1)} %bitcast.87, bf16[1,2048,512]{2,1,0:T(8,128)(2,1)S(1)} %copy-done.24), kind=kOutput, calls=%fused_computation.22 | convolution fusion | flops 2150629376 | bytes 9437184 | tf_op jit(solution)/shard_map/dot_general | solution.py:121
  118.5 1.8 convert_multiply_fusion.4
  125.8 2.0 multiply_add_fusion.1
  127.8 1.6 slice.283
  129.4 1.6 slice.284
  132.4 1.8 multiply_add_fusion.2
  135.5 1.5 slice.288
  137.0 1.5 slice.292
  138.6 1.6 multiply_add_fusion.3
  178.7 1.5 slice.287
  182.9 1.6 slice.330
  199.8 1.7 pad.114
  201.7 1.9 fusion.39
  204.4 12.8 %all-gather.1 = f32[8,1,512]{2,1,0:T(1,128)S(1)} all-gather(f32[1,1,512]{2,1,0:T(1,128)S(1)} %add_bitcast_fusion), channel_id=1, replica_groups=mesh['ep'=8,'tp'=4] {'ep'}, dimensions={0}, use_global_device_ids=true | all-gather | bytes 18432 | tf_op jit(solution)/shard_map/all_gather | solution.py:18
  217.2 1.7 pad.130
  218.9 1.6 pad.129
  221.3 12.8 %all-gather = f32[8,1,512]{2,1,0:T(1,128)S(1)} all-gather(f32[1,1,512]{2,1,0:T(1,128)S(1)} %add_bitcast_fusion.1), channel_id=1, replica_groups=mesh['ep'=8,'tp'=4] {'ep'}, dimensions={0}, use_global_device_ids=true | all-gather | bytes 18432 | tf_op jit(solution)/shard_map/all_gather | solution.py:18
  234.1 6.2 %fusion.14 = bf16[1024,512]{1,0:T(8,128)(2,1)} fusion(bf16[1024,2048]{1,0:T(8,128)(2,1)} %all-gather.7.cloned.1.call-done, bf16[1,2048,512]{2,1,0:T(8,128)(2,1)} %param.33), kind=kOutput, calls=%fused_computation.23 | convolution fusion | flops 2148007936 | bytes 7340032 | tf_op jit(solution)/shard_map/dot_general | solution.py:125
  240.3 3.9 %all-to-all-start.1 = ((bf16[8,128,512]{2,1,0:T(8,128)(2,1)}), bf16[8,128,512]{2,1,0:T(8,128)(2,1)S(1)}, u32[]{:S(2)}, u32[]{:S(2)}) async-start(bf16[8,128,512]{2,1,0:T(8,128)(2,1)} %bitcast.72), calls=%async_computation.1 | async-start | bytes 2097152 | tf_op jit(solution)/shard_map/all_to_all | solution.py:131
  244.7 4.1 %fusion.32 = bf16[256,512]{1,0:T(8,128)(2,1)} fusion(bf16[2048,512]{1,0:T(8,128)(2,1)} %param.21, f32[256,512]{1,0:T(8,128)} %pad.129, f32[256,512]{1,0:T(8,128)} %pad.130, f32[256,512]{1,0:T(8,128)} %copy-done.4, f32[256,512]{1,0:T(8,128)} %pad.114, bf16[256,2048]{1,0:T(8,128)(2,1)} %param.18, f32[2048]{0:T(1024)S(1)} %copy-done.28, ...), kind=kOutput, calls=%fused_computation.45 | convolution fusion | flops 541065216 | bytes 5516288 | tf_op jit(solution)/shard_map/dot_general | solution.py:68
  248.8 21.7 %all-to-all-done.1 = bf16[8,128,512]{2,1,0:T(8,128)(2,1)S(1)} async-done(((bf16[8,128,512]{2,1,0:T(8,128)(2,1)}), bf16[8,128,512]{2,1,0:T(8,128)(2,1)S(1)}, u32[]{:S(2)}, u32[]{:S(2)}) %all-to-all-start.1) | async-done | bytes 1048608 | tf_op jit(solution)/shard_map/all_to_all | solution.py:131
  270.5 2.6 gather_fusion.1
  273.1 1.7 reshape.120
  274.8 2.1 multiply_reduce_fusion
  (229 shorter events, 79.7 us)
Async XLA Ops:
  7.2 100.3 %copy-start = (bf16[1,2048,512]{2,1,0:T(8,128)(2,1)S(1)}, bf16[1,2048,512]{2,1,0:T(8,128)(2,1)}, u32[]{:S(2)}) copy-start(bf16[1,2048,512]{2,1,0:T(8,128)(2,1)} %param.32) | copy-start | bytes 6291460
  7.2 8.0 %copy-start.1 = (bf16[256,2048]{1,0:T(8,128)(2,1)S(1)}, bf16[256,2048]{1,0:T(8,128)(2,1)}, u32[]{:S(2)}) copy-start(bf16[256,2048]{1,0:T(8,128)(2,1)} %param.27) | copy-start | bytes 3145732
  7.2 8.0 %copy-start.12 = (f32[2048]{0:T(1024)S(1)}, f32[2048]{0:T(1024)}, u32[]{:S(2)}) copy-start(f32[2048]{0:T(1024)} %param.28) | copy-start | bytes 24580
  7.2 100.2 %all-gather.5.cloned.1.call-start = ((), (), s32[]{:S(2)}) async-start(), calls=%async_computation.2 | async-start | bytes 5242880 | tf_op jit(solution)/shard_map/all_gather | solution.py:117
  22.9 33.1 %copy-start.2 = (bf16[256,2048]{1,0:T(8,128)(2,1)S(1)}, bf16[256,2048]{1,0:T(8,128)(2,1)}, u32[]{:S(2)}) copy-start(bf16[256,2048]{1,0:T(8,128)(2,1)} %param.18) | copy-start | bytes 3145732
  22.9 33.9 %copy-start.27 = (f32[2048]{0:T(1024)S(1)}, f32[2048]{0:T(1024)}, u32[]{:S(2)}) copy-start(f32[2048]{0:T(1024)} %param.19) | copy-start | bytes 24580
  55.9 178.2 %all-gather.7.cloned.1.call-start = ((), (), s32[]{:S(2)}) async-start(), calls=%async_computation.3 | async-start | bytes 5242880 | tf_op jit(solution)/shard_map/all_gather | solution.py:126
  56.8 4.7 %copy-start.18 = (f32[256,2]{0,1:T(2,128)S(1)}, f32[256,2]{0,1:T(2,128)}, u32[]{:S(2)}) copy-start(f32[256,2]{0,1:T(2,128)} %param.30) | copy-start | bytes 6148
  56.8 4.7 %copy-start.20 = (f32[512]{0:T(512)S(1)}, f32[512]{0:T(512)}, u32[]{:S(2)}) copy-start(f32[512]{0:T(512)} %param.25) | copy-start | bytes 6148
  56.8 4.7 %copy-start.19 = (f32[4,512]{1,0:T(4,128)S(1)}, f32[4,512]{1,0:T(4,128)}, u32[]{:S(2)}) copy-start(f32[4,512]{1,0:T(4,128)} %param.22) | copy-start | bytes 24580
  59.2 0.7 copy-start.7
  59.9 3.0 %collective-permute-start = (bf16[3,512]{1,0:T(4,128)(2,1)S(1)}, bf16[3,512]{1,0:T(4,128)(2,1)S(1)}, u32[]{:S(2)}, u32[]{:S(2)}) collective-permute-start(bf16[3,512]{1,0:T(4,128)(2,1)S(1)} %slice.356), channel_id=1, source_target_pairs={{0,4},{4,8},{8,12},{12,16},{16,20},{20,24},{24,28},{1,5},{5,9},{9,... | collective-permute-start | bytes 9224 | tf_op jit(solution)/shard_map/ppermute | solution.py:13
  107.4 4.7 %copy-start.23 = (bf16[8,128,2048]{2,1,0:T(8,128)(2,1)S(1)}, bf16[8,128,2048]{2,1,0:T(8,128)(2,1)}, u32[]{:S(2)}) copy-start(bf16[8,128,2048]{2,1,0:T(8,128)(2,1)} %all-gather.5.cloned.1.call-done) | copy-start | bytes 12582916
  107.4 4.7 %copy-start.24 = (bf16[1,2048,512]{2,1,0:T(8,128)(2,1)S(1)}, bf16[1,2048,512]{2,1,0:T(8,128)(2,1)}, u32[]{:S(2)}) copy-start(bf16[1,2048,512]{2,1,0:T(8,128)(2,1)} %param.31) | copy-start | bytes 6291460
  112.1 3.7 %copy-start.25 = (bf16[4,128,128]{2,1,0:T(8,128)(2,1)S(1)}, bf16[4,128,128]{2,1,0:T(8,128)(2,1)}, u32[]{:S(2)}) copy-start(bf16[4,128,128]{2,1,0:T(8,128)(2,1)} %param.23) | copy-start | bytes 393220
  115.8 1.4 copy-start.26
  186.4 12.3 %copy-start.8 = (f32[31,512]{1,0:T(8,128)S(1)}, f32[31,512]{1,0:T(8,128)}, u32[]{:S(2)}) copy-start(f32[31,512]{1,0:T(8,128)} %slice.287) | copy-start | bytes 190468
  186.4 12.3 %copy-start.9 = (f32[31,512]{1,0:T(8,128)S(1)}, f32[31,512]{1,0:T(8,128)}, u32[]{:S(2)}) copy-start(f32[31,512]{1,0:T(8,128)} %slice.328) | copy-start | bytes 190468
  189.8 9.0 %copy-start.17 = (f32[1,512]{1,0:T(1,128)S(1)}, f32[1,512]{1,0:T(1,128)}, u32[]{:S(2)}) copy-start(f32[1,512]{1,0:T(1,128)} %slice.389) | copy-start | bytes 6148
  194.2 5.4 %copy-start.6 = (f32[63,512]{1,0:T(8,128)S(1)}, f32[63,512]{1,0:T(8,128)}, u32[]{:S(2)}) copy-start(f32[63,512]{1,0:T(8,128)} %slice.330) | copy-start | bytes 387076
  197.9 1.8 copy-start.16
  199.5 2.0 copy-start.15
  201.5 2.1 copy-start.14
  201.7 17.2 %copy-start.13 = (f32[1,512]{1,0:T(1,128)S(1)}, f32[1,512]{1,0:T(1,128)}, u32[]{:S(2)}) copy-start(f32[1,512]{1,0:T(1,128)} %slice.387) | copy-start | bytes 6148
  203.6 15.3 %copy-start.3 = (f32[127,512]{1,0:T(8,128)S(1)}, f32[127,512]{1,0:T(8,128)}, u32[]{:S(2)}) copy-start(f32[127,512]{1,0:T(8,128)} %get-tuple-element.130) | copy-start | bytes 780292
  203.7 36.6 %copy-start.4 = (f32[256,512]{1,0:T(8,128)}, f32[256,512]{1,0:T(8,128)S(1)}, u32[]{:S(2)}) copy-start(f32[256,512]{1,0:T(8,128)S(1)} %pad.113) | copy-start | bytes 1572868
  240.3 3.9 %copy-start.10 = (f32[512]{0:T(512)S(1)}, f32[512]{0:T(512)}, u32[]{:S(2)}) copy-start(f32[512]{0:T(512)} %custom-call) | copy-start | bytes 6148
  240.3 4.4 %copy-start.22 = (f32[256]{0:T(256)S(1)}, f32[256]{0:T(256)}, u32[]{:S(2)}) copy-start(f32[256]{0:T(256)} %copy-done.21) | copy-start | bytes 3076
  240.3 4.4 %copy-start.28 = (f32[2048]{0:T(1024)S(1)}, f32[2048]{0:T(1024)}, u32[]{:S(2)}) copy-start(f32[2048]{0:T(1024)} %param.19) | copy-start | bytes 24580
  240.3 30.2 %all-to-all-start.1 = ((bf16[8,128,512]{2,1,0:T(8,128)(2,1)}), bf16[8,128,512]{2,1,0:T(8,128)(2,1)S(1)}, u32[]{:S(2)}, u32[]{:S(2)}) async-start(bf16[8,128,512]{2,1,0:T(8,128)(2,1)} %bitcast.72), calls=%async_computation.1 | async-start | bytes 2097152 | tf_op jit(solution)/shard_map/all_to_all | solution.py:131
  244.7 25.8 %copy-start.11 = (s32[1024]{0:T(1024)S(1)}, s32[1024]{0:T(1024)}, u32[]{:S(2)}) copy-start(s32[1024]{0:T(1024)} %pad_clamp_fusion) | copy-start | bytes 12292
  270.5 4.3 %copy-start.5 = (f32[256,2]{1,0:T(8,128)S(1)}, f32[256,2]{1,0:T(8,128)}, u32[]{:S(2)}) copy-start(f32[256,2]{1,0:T(8,128)} %copy.41) | copy-start | bytes 6148
  (1 other events, 0.6 us)
Sparse Core Ops, SparseCore 0:
  56.0 51.3 all-gather.4
  115.9 52.4 all-gather.6
where the time goes:
time: 286 us; the launch traced here: 284 us
  local copies, waits for them, and re-layouts  86.2 us (30%)
  waiting for transfers between devices  64.5 us (23%)
  blocking collectives  58.5 us (20%)
  other arithmetic  32.3 us (11%)
  matrix products  21.7 us (8%)
  between operations  14.8 us (5%)
  starting transfers between devices  5.54 us (2%)
    slice x52, local copies, waits for them, and re-layouts, local(): lax.associative_scan(link, (jnp.exp(log_decay), lru_drive), axis=0)  60.4 us
    all_gather x1, waiting for transfers between devices, local(): piece = lax.all_gather(incoming, 'tp', axis=2, tiled=True)  42.8 us
    all_to_all x1, blocking collectives, local(): lax.all_to_all(own_columns, 'ep', split_axis=0, concat_axis=0, tiled=True)  33 us
    all_gather x2, blocking collectives, entering(): everything = jax.tree.map(lambda part: lax.all_gather(part, axis), value)  25.6 us
    all_to_all x1, waiting for transfers between devices, local(): lax.all_to_all(results, 'ep', split_axis=0, concat_axis=0, tiled=True)  21.7 us
    add x13, other arithmetic, link(): return (earlier[0] * later[0], later[0] * earlier[1] + later[1])  14.6 us
    dot_general x1, matrix products, local(): jnp.dot(lax.all_gather(hidden, 'tp', axis=1, tiled=True), down_rows, pref...  6.22 us
    gather x1, local copies, waits for them, and re-layouts, local(): padded_rows[slot_owner].reshape(expert_count, capacity, feature_count)  5.98 us
  transfers between devices with their start and end apart: 4, of which 2 were waited for; matrix products, arithmetic and copies ran while one was open for 36% of the time, Pallas kernels for 0%

commit v1 on v0

--- a/solution.py
+++ b/solution.py
@@ -114,7 +114,7 @@
         outgoing, lax.axis_index("tp") * column_width, column_width, 2
     )
     incoming = lax.all_to_all(own_columns, "ep", split_axis=0, concat_axis=0, tiled=True)
-    piece = lax.all_gather(incoming, "tp", axis=2, tiled=True)
+    piece = jnp.concatenate(lax.all_gather(incoming, "tp"), axis=2)
     flat_rows = piece.reshape(slot_total, piece.shape[2])
     gate_rows = expert_gate[0]
     up_rows = expert_up[0]

time: 286 us -> 294 us (1.028)
  local copies, waits for them, and re-layouts: 86.2 us -> 93.8 us
    reshape x0 -> x1, local copies, waits for them, and re-layouts: none -> 7.54 us  [local(): piece = jnp.concatenate(lax.all_gather(incoming, 'tp'), axis=2)]
  transfers between devices with their start and end apart: 4 -> 4, of which waited for: 2 -> 2; matrix products, arithmetic and copies ran while one was open for 36% -> 35% of each run, Pallas kernels for 0% -> 0%
where the time goes in v1:
time: 294 us; the launch traced here: 291 us
  local copies, waits for them, and re-layouts  93.8 us (32%)
  waiting for transfers between devices  64.4 us (22%)
  blocking collectives  58.5 us (20%)
  other arithmetic  32.4 us (11%)
  matrix products  21.7 us (7%)
  between operations  14.8 us (5%)
  starting transfers between devices  5.53 us (2%)
    slice x52, local copies, waits for them, and re-layouts, local(): lax.associative_scan(link, (jnp.exp(log_decay), lru_drive), axis=0)  60.4 us
    all_gather x1, waiting for transfers between devices, local(): piece = jnp.concatenate(lax.all_gather(incoming, 'tp'), axis=2)  42.7 us
    all_to_all x1, blocking collectives, local(): lax.all_to_all(own_columns, 'ep', split_axis=0, concat_axis=0, tiled=True)  33 us
    all_gather x2, blocking collectives, entering(): everything = jax.tree.map(lambda part: lax.all_gather(part, axis), value)  25.6 us
    all_to_all x1, waiting for transfers between devices, local(): lax.all_to_all(results, 'ep', split_axis=0, concat_axis=0, tiled=True)  21.7 us
    add x13, other arithmetic, link(): return (earlier[0] * later[0], later[0] * earlier[1] + later[1])  14.6 us
    reshape x1, local copies, waits for them, and re-layouts, local(): piece = jnp.concatenate(lax.all_gather(incoming, 'tp'), axis=2)  7.54 us
    dot_general x1, matrix products, local(): jnp.dot(lax.all_gather(hidden, 'tp', axis=1, tiled=True), down_rows, pref...  6.24 us
  transfers between devices with their start and end apart: 4, of which 2 were waited for; matrix products, arithmetic and copies ran while one was open for 35% of the time, Pallas kernels for 0%

profile of v1, /device:TPU:0, one launch (start us, length us, event | category | flops | bytes accessed | tf_op | source)
XLA Modules:
  0.0 291.4 jit_solution(12454474005135494210)
XLA Ops:
  11.2 2.4 scatter_custom_fusion
  15.6 6.0 %gather_fusion = bf16[1024,2048]{1,0:T(8,128)(2,1)} fusion(bf16[257,2048]{1,0:T(8,128)(2,1)S(1)} %concatenate.63, s32[1024]{0:T(1024)S(1)} %fusion.56), kind=kCustom, calls=%fused_computation | custom fusion | bytes 8392704 | tf_op jit(solution)/shard_map/gather | solution.py:111
  22.9 33.0 %all_to_all.10 = bf16[8,128,512]{2,1,0:T(8,128)(2,1)} all-to-all(bf16[8,128,512]{2,1,0:T(8,128)(2,1)S(1)} %constant_dynamic-slice_fusion.2), channel_id=1, replica_groups=mesh['ep'=8,'tp'=4] {'ep'}, dimensions={0} | all-to-all | bytes 2097152 | tf_op jit(solution)/shard_map/all_to_all | solution.py:116
  56.8 2.4 convolution_convert_fusion.1
  63.0 1.9 add_convert_fusion
  64.8 42.7 %all-gather.8.cloned.1.call-done = bf16[32,128,512]{2,1,0:T(8,128)(2,1)} async-done(((bf16[8,128,512]{2,1,0:T(8,128)(2,1)}), bf16[32,128,512]{2,1,0:T(8,128)(2,1)}) %all-gather.8.cloned.1.call-update) | async-done | bytes 4194320 | tf_op jit(solution)/shard_map/all_gather | solution.py:117
  107.5 7.5 %copy.56 = bf16[8,128,4,512]{1,0,3,2:T(8,128)(2,1)} copy(bf16[8,128,4,512]{3,1,0,2:T(8,128)(2,1)} %bitcast.83) | data formatting | bytes 8388608 | tf_op jit(solution)/shard_map/reshape | solution.py:117
  115.1 4.7 %fusion.2 = f32[1024,512]{1,0:T(8,128)S(1)} fusion(bf16[256,8,8,128]{3,2,1,0:T(8,128)(2,1)} %bitcast.84, bf16[1,2048,512]{2,1,0:T(8,128)(2,1)S(1)} %copy-done), kind=kOutput, calls=%fused_computation.8 | convolution fusion | flops 2147483648 | bytes 8388608 | tf_op jit(solution)/shard_map/dot_general | solution.py:121
  119.8 3.6 %multiply_convert_fusion = bf16[1024,512]{1,0:T(8,128)(2,1)} fusion(f32[1024,512]{1,0:T(8,128)S(1)} %fusion.2, bf16[1,2048,512]{2,1,0:T(8,128)(2,1)S(1)} %copy-done.24, bf16[256,8,8,128]{3,2,1,0:T(8,128)(2,1)S(1)} %bitcast.85), kind=kOutput, calls=%fused_computation.26 | convolution fusion | flops 2150629376 | bytes 9437184 | tf_op jit(solution)/shard_map/dot_general | solution.py:122
  126.2 1.8 convert_multiply_fusion.4
  133.5 2.0 multiply_add_fusion.1
  135.5 1.6 slice.283
  137.1 1.6 slice.284
  140.1 1.8 multiply_add_fusion.2
  143.1 1.5 slice.288
  144.7 1.5 slice.292
  146.2 1.6 multiply_add_fusion.3
  186.3 1.5 slice.287
  190.6 1.6 slice.330
  207.5 1.7 pad.114
  209.3 1.9 fusion.45
  212.1 12.8 %all-gather.2 = f32[8,1,512]{2,1,0:T(1,128)S(1)} all-gather(f32[1,1,512]{2,1,0:T(1,128)S(1)} %add_bitcast_fusion), channel_id=1, replica_groups=mesh['ep'=8,'tp'=4] {'ep'}, dimensions={0}, use_global_device_ids=true | all-gather | bytes 18432 | tf_op jit(solution)/shard_map/all_gather | solution.py:18
  224.9 1.7 pad.130
  226.6 1.6 pad.129
  229.0 12.8 %all-gather.1 = f32[8,1,512]{2,1,0:T(1,128)S(1)} all-gather(f32[1,1,512]{2,1,0:T(1,128)S(1)} %add_bitcast_fusion.1), channel_id=1, replica_groups=mesh['ep'=8,'tp'=4] {'ep'}, dimensions={0}, use_global_device_ids=true | all-gather | bytes 18432 | tf_op jit(solution)/shard_map/all_gather | solution.py:18
  241.8 6.2 %fusion.20 = bf16[1024,512]{1,0:T(8,128)(2,1)} fusion(bf16[1024,2048]{1,0:T(8,128)(2,1)} %all-gather.6.cloned.1.call-done, bf16[1,2048,512]{2,1,0:T(8,128)(2,1)} %param.33), kind=kOutput, calls=%fused_computation.27 | convolution fusion | flops 2148007936 | bytes 7340032 | tf_op jit(solution)/shard_map/dot_general | solution.py:125
  248.0 3.9 %all-to-all-start.1 = ((bf16[8,128,512]{2,1,0:T(8,128)(2,1)}), bf16[8,128,512]{2,1,0:T(8,128)(2,1)S(1)}, u32[]{:S(2)}, u32[]{:S(2)}) async-start(bf16[8,128,512]{2,1,0:T(8,128)(2,1)} %bitcast.86), calls=%async_computation.1 | async-start | bytes 2097152 | tf_op jit(solution)/shard_map/all_to_all | solution.py:131
  252.4 4.1 %fusion.38 = bf16[256,512]{1,0:T(8,128)(2,1)} fusion(bf16[2048,512]{1,0:T(8,128)(2,1)} %param.21, f32[256,512]{1,0:T(8,128)} %pad.129, f32[256,512]{1,0:T(8,128)} %pad.130, f32[256,512]{1,0:T(8,128)} %copy-done.5, f32[256,512]{1,0:T(8,128)} %pad.114, bf16[256,2048]{1,0:T(8,128)(2,1)} %param.18, f32[2048]{0:T(1024)S(1)} %copy-done.28, ...), kind=kOutput, calls=%fused_computation.49 | convolution fusion | flops 541065216 | bytes 5516288 | tf_op jit(solution)/shard_map/dot_general | solution.py:68
  256.5 21.7 %all-to-all-done.1 = bf16[8,128,512]{2,1,0:T(8,128)(2,1)S(1)} async-done(((bf16[8,128,512]{2,1,0:T(8,128)(2,1)}), bf16[8,128,512]{2,1,0:T(8,128)(2,1)S(1)}, u32[]{:S(2)}, u32[]{:S(2)}) %all-to-all-start.1) | async-done | bytes 1048608 | tf_op jit(solution)/shard_map/all_to_all | solution.py:131
  278.2 2.6 gather_fusion.1
  280.8 1.7 reshape.120
  282.5 2.1 multiply_reduce_fusion
  (230 shorter events, 81.3 us)
Async XLA Ops:
  7.2 107.9 %copy-start = (bf16[1,2048,512]{2,1,0:T(8,128)(2,1)S(1)}, bf16[1,2048,512]{2,1,0:T(8,128)(2,1)}, u32[]{:S(2)}) copy-start(bf16[1,2048,512]{2,1,0:T(8,128)(2,1)} %param.31) | copy-start | bytes 6291460
  7.2 8.0 %copy-start.2 = (bf16[256,2048]{1,0:T(8,128)(2,1)S(1)}, bf16[256,2048]{1,0:T(8,128)(2,1)}, u32[]{:S(2)}) copy-start(bf16[256,2048]{1,0:T(8,128)(2,1)} %param.27) | copy-start | bytes 3145732
  7.2 8.0 %copy-start.13 = (f32[2048]{0:T(1024)S(1)}, f32[2048]{0:T(1024)}, u32[]{:S(2)}) copy-start(f32[2048]{0:T(1024)} %param.28) | copy-start | bytes 24580
  7.2 100.3 %all-gather.8.cloned.1.call-start = ((), (), s32[]{:S(2)}) async-start(), calls=%async_computation.3 | async-start | bytes 5242880 | tf_op jit(solution)/shard_map/all_gather | solution.py:117
  22.9 33.1 %copy-start.3 = (bf16[256,2048]{1,0:T(8,128)(2,1)S(1)}, bf16[256,2048]{1,0:T(8,128)(2,1)}, u32[]{:S(2)}) copy-start(bf16[256,2048]{1,0:T(8,128)(2,1)} %param.18) | copy-start | bytes 3145732
  22.9 33.9 %copy-start.27 = (f32[2048]{0:T(1024)S(1)}, f32[2048]{0:T(1024)}, u32[]{:S(2)}) copy-start(f32[2048]{0:T(1024)} %param.19) | copy-start | bytes 24580
  55.9 185.9 %all-gather.6.cloned.1.call-start = ((), (), s32[]{:S(2)}) async-start(), calls=%async_computation.2 | async-start | bytes 5242880 | tf_op jit(solution)/shard_map/all_gather | solution.py:126
  56.8 4.7 %copy-start.19 = (f32[256,2]{0,1:T(2,128)S(1)}, f32[256,2]{0,1:T(2,128)}, u32[]{:S(2)}) copy-start(f32[256,2]{0,1:T(2,128)} %param.30) | copy-start | bytes 6148
  56.8 4.7 %copy-start.21 = (f32[512]{0:T(512)S(1)}, f32[512]{0:T(512)}, u32[]{:S(2)}) copy-start(f32[512]{0:T(512)} %param.25) | copy-start | bytes 6148
  56.8 4.7 %copy-start.20 = (f32[4,512]{1,0:T(4,128)S(1)}, f32[4,512]{1,0:T(4,128)}, u32[]{:S(2)}) copy-start(f32[4,512]{1,0:T(4,128)} %param.22) | copy-start | bytes 24580
  59.2 0.7 copy-start.8
  59.9 3.0 %collective-permute-start = (bf16[3,512]{1,0:T(4,128)(2,1)S(1)}, bf16[3,512]{1,0:T(4,128)(2,1)S(1)}, u32[]{:S(2)}, u32[]{:S(2)}) collective-permute-start(bf16[3,512]{1,0:T(4,128)(2,1)S(1)} %slice.356), channel_id=1, source_target_pairs={{0,4},{4,8},{8,12},{12,16},{16,20},{20,24},{24,28},{1,5},{5,9},{9,... | collective-permute-start | bytes 9224 | tf_op jit(solution)/shard_map/ppermute | solution.py:13
  115.1 4.7 %copy-start.1 = (bf16[8,128,4,512]{1,0,3,2:T(8,128)(2,1)S(1)}, bf16[8,128,4,512]{1,0,3,2:T(8,128)(2,1)}, u32[]{:S(2)}) copy-start(bf16[8,128,4,512]{1,0,3,2:T(8,128)(2,1)} %copy.56) | copy-start | bytes 12582916
  115.1 4.7 %copy-start.24 = (bf16[1,2048,512]{2,1,0:T(8,128)(2,1)S(1)}, bf16[1,2048,512]{2,1,0:T(8,128)(2,1)}, u32[]{:S(2)}) copy-start(bf16[1,2048,512]{2,1,0:T(8,128)(2,1)} %param.32) | copy-start | bytes 6291460
  119.8 3.7 %copy-start.25 = (bf16[4,128,128]{2,1,0:T(8,128)(2,1)S(1)}, bf16[4,128,128]{2,1,0:T(8,128)(2,1)}, u32[]{:S(2)}) copy-start(bf16[4,128,128]{2,1,0:T(8,128)(2,1)} %param.23) | copy-start | bytes 393220
  123.4 1.4 copy-start.26
  194.1 12.3 %copy-start.9 = (f32[31,512]{1,0:T(8,128)S(1)}, f32[31,512]{1,0:T(8,128)}, u32[]{:S(2)}) copy-start(f32[31,512]{1,0:T(8,128)} %slice.287) | copy-start | bytes 190468
  194.1 12.3 %copy-start.10 = (f32[31,512]{1,0:T(8,128)S(1)}, f32[31,512]{1,0:T(8,128)}, u32[]{:S(2)}) copy-start(f32[31,512]{1,0:T(8,128)} %slice.328) | copy-start | bytes 190468
  197.4 9.0 %copy-start.18 = (f32[1,512]{1,0:T(1,128)S(1)}, f32[1,512]{1,0:T(1,128)}, u32[]{:S(2)}) copy-start(f32[1,512]{1,0:T(1,128)} %slice.389) | copy-start | bytes 6148
  201.9 5.4 %copy-start.7 = (f32[63,512]{1,0:T(8,128)S(1)}, f32[63,512]{1,0:T(8,128)}, u32[]{:S(2)}) copy-start(f32[63,512]{1,0:T(8,128)} %slice.330) | copy-start | bytes 387076
  205.6 1.8 copy-start.17
  207.2 2.0 copy-start.16
  209.2 2.1 copy-start.15
  209.3 17.2 %copy-start.14 = (f32[1,512]{1,0:T(1,128)S(1)}, f32[1,512]{1,0:T(1,128)}, u32[]{:S(2)}) copy-start(f32[1,512]{1,0:T(1,128)} %slice.387) | copy-start | bytes 6148
  211.2 15.3 %copy-start.4 = (f32[127,512]{1,0:T(8,128)S(1)}, f32[127,512]{1,0:T(8,128)}, u32[]{:S(2)}) copy-start(f32[127,512]{1,0:T(8,128)} %get-tuple-element.130) | copy-start | bytes 780292
  211.3 36.6 %copy-start.5 = (f32[256,512]{1,0:T(8,128)}, f32[256,512]{1,0:T(8,128)S(1)}, u32[]{:S(2)}) copy-start(f32[256,512]{1,0:T(8,128)S(1)} %pad.113) | copy-start | bytes 1572868
  248.0 3.9 %copy-start.11 = (f32[512]{0:T(512)S(1)}, f32[512]{0:T(512)}, u32[]{:S(2)}) copy-start(f32[512]{0:T(512)} %custom-call) | copy-start | bytes 6148
  248.0 4.4 %copy-start.23 = (f32[256]{0:T(256)S(1)}, f32[256]{0:T(256)}, u32[]{:S(2)}) copy-start(f32[256]{0:T(256)} %copy-done.22) | copy-start | bytes 3076
  248.0 4.4 %copy-start.28 = (f32[2048]{0:T(1024)S(1)}, f32[2048]{0:T(1024)}, u32[]{:S(2)}) copy-start(f32[2048]{0:T(1024)} %param.19) | copy-start | bytes 24580
  248.0 30.2 %all-to-all-start.1 = ((bf16[8,128,512]{2,1,0:T(8,128)(2,1)}), bf16[8,128,512]{2,1,0:T(8,128)(2,1)S(1)}, u32[]{:S(2)}, u32[]{:S(2)}) async-start(bf16[8,128,512]{2,1,0:T(8,128)(2,1)} %bitcast.86), calls=%async_computation.1 | async-start | bytes 2097152 | tf_op jit(solution)/shard_map/all_to_all | solution.py:131
  252.4 25.8 %copy-start.12 = (s32[1024]{0:T(1024)S(1)}, s32[1024]{0:T(1024)}, u32[]{:S(2)}) copy-start(s32[1024]{0:T(1024)} %pad_clamp_fusion) | copy-start | bytes 12292
  278.2 4.3 %copy-start.6 = (f32[256,2]{1,0:T(8,128)S(1)}, f32[256,2]{1,0:T(8,128)}, u32[]{:S(2)}) copy-start(f32[256,2]{1,0:T(8,128)} %copy.52) | copy-start | bytes 6148
  (1 other events, 0.6 us)
Sparse Core Ops, SparseCore 0:
  56.0 51.4 all-gather.7
  123.6 52.4 all-gather.5
